TPU v7x, 512 devices: a whole 4x8x8 slice. The times are simulated.
512 devices in a mesh: sp: 32 (over z, x), tp: 16 (over y, core).
Axes of the slice: x: 4, y: 8, z: 8, core: 2. Of those that a mesh axis runs over, the one named last changes fastest.
Arguments:
- queries: bfloat16 [8192, 2048], P('sp', 'tp'), may hold values from -6 to 6
- key_matrix: bfloat16 [8192, 2048], P('sp', 'tp'), may hold values from -6 to 6
- value_matrix: bfloat16 [8192, 4096], P('sp', 'tp'), may hold values from -6 to 6
- output_gate_preactivation: bfloat16 [8192, 4096], P('sp', 'tp'), may hold values from -6 to 6
- decay_preactivation: bfloat16 [8192, 2048], P('sp', 'tp')
- extra_log_decay: float32 [8192, 16], P('sp', 'tp'), may hold values from -0.7 to 0
- head_norm_gain: bfloat16 [256], replicated, may hold values from 0.099609375 to 1.8984375
- output_projection: bfloat16 [4096, 2048], P(None, 'tp'), may hold values from -0.09375 to 0.09375
- residual: bfloat16 [8192, 2048], P('sp', 'tp'), may hold values from -210 to 210
- feedforward_gain: bfloat16 [2048], replicated, may hold values from 0.099609375 to 1.8984375
- routing: int32 [8192, 4], P('sp'), may hold values from 0 to 127, all different within a row; in each aligned block of 256 rows (0 to 255, 256 to 511, ...) at most 12 rows name the same one
- router_score: float32 [8192, 4], P('sp'), may hold values from 0.05 to 1
- expert_gate_weight: bfloat16 [2048, 131072], P(None, ('sp', 'tp')), may hold values from -0.125 to 0.125
- expert_up_weight: bfloat16 [2048, 131072], P(None, ('sp', 'tp')), may hold values from -0.125 to 0.125
- expert_down_weight: bfloat16 [131072, 2048], P(('sp', 'tp')), may hold values from -0.1875 to 0.1875
- shared_expert_gate: bfloat16 [2048, 512], P(None, 'tp'), may hold values from -0.125 to 0.125
- shared_expert_up: bfloat16 [2048, 512], P(None, 'tp'), may hold values from -0.125 to 0.125
- shared_expert_down: bfloat16 [512, 2048], P(None, 'tp'), may hold values from -0.25 to 0.25
Outputs:
- layer_out: bfloat16 [8192, 2048], P('sp', 'tp')
Inputs may be any that keep to these rules, and one draw needn't show every extreme that they name: `routing`: each row names 4 different experts. In each aligned block of 256 rows, the rows of one index of sp, no expert is named by more than 12 rows, a bound that some expert reaches in some blocks.
All inputs are finite; a program needn't handle non-finite values.
Results may differ from a plain program's by a relative error of at most 0.01.
Values may be sent and summed in bfloat16 or wider, within the bound.
No kernel may reach another device: no remote copies, remote signals or barrier semaphores. Data moves between devices by JAX's collectives and lax.ppermute only.
A program may use at most 64 MiB of HBM per device.

v0:
```python
import jax
import jax.numpy as jnp
from jax import lax
from jax.sharding import Mesh
from jax.sharding import PartitionSpec as P

DK = 128
DV = 256
BLOCK_POSITIONS = 64
FF_PARTS = 4
SP = ("sp_0", "sp_1")
SP_TP = ("sp_0", "sp_1", "tp")
HIGHEST = lax.Precision.HIGHEST
EPSILON = 1e-06
ROUTE_SCALE = 2.5
GATE_TEMPER = 16.0


def nothing_yet(value, identity):
    return jax.tree.map(
        lambda part, zero: jnp.zeros_like(part) + jnp.asarray(zero, part.dtype), value, identity
    )


def prefix_by_axis(value, axes, combine, identity):
    before = start = nothing_yet(value, identity)
    total = value
    for axis in reversed(axes):
        count, position = (lax.axis_size(axis), lax.axis_index(axis))
        pieces = jax.tree.map(
            lambda part, kind: lax.all_gather(part.astype(kind), axis),
            total,
            (jnp.bfloat16, jnp.bfloat16),
        )
        inside, total = (start, start)
        for k in range(count):
            passed = k < position
            total = combine(
                total, jax.tree.map(lambda part, own: part[k].astype(own.dtype), pieces, value)
            )
            inside = jax.tree.map(lambda new, old: jnp.where(passed, new, old), total, inside)
        before = combine(inside, before)
    return before


def laid_out(blocks, dim):
    blocks = jnp.moveaxis(blocks, 0, dim)
    dims = blocks.shape
    return blocks.reshape(*dims[:dim], dims[dim] * dims[dim + 1], *dims[dim + 2 :])


def sent_to_all(value, axis):
    copies = jnp.broadcast_to(value, (lax.axis_size(axis), *value.shape))
    return lax.all_to_all(copies, axis, split_axis=0, concat_axis=0, tiled=True)


def gather_directly(value, axis, dim):
    return laid_out(sent_to_all(value, axis), dim)


def from_partner(value, axis, bit):
    mask = 2**bit
    pairs = [(source, source ^ mask) for source in range(lax.axis_size(axis))]
    return lax.ppermute(value, axis, pairs)


def carry_combine(first_part, second_part):
    return (
        first_part[0] * second_part[0],
        second_part[0][..., None] * first_part[1] + second_part[1],
    )


def attention_heads(queries, key_matrix, value_matrix, decay_preactivation, extra_log_decay):
    tokens = queries.shape[0]
    local_head_count = extra_log_decay.shape[1]
    block_count = tokens // BLOCK_POSITIONS
    query_block = queries.astype(jnp.float32).reshape(
        block_count, BLOCK_POSITIONS, local_head_count, DK
    ) * DK ** (-0.5)
    key_block = key_matrix.astype(jnp.float32).reshape(
        block_count, BLOCK_POSITIONS, local_head_count, DK
    )
    value_block = value_matrix.astype(jnp.float32).reshape(
        block_count, BLOCK_POSITIONS, local_head_count, DV
    )
    log_decay_rows = (
        jax.nn.log_sigmoid(decay_preactivation.astype(jnp.float32)).reshape(
            block_count, BLOCK_POSITIONS, local_head_count, DK
        )
        / GATE_TEMPER
    )
    log_decay_rows = (
        log_decay_rows
        + extra_log_decay.reshape(block_count, BLOCK_POSITIONS, local_head_count)[..., None]
    )
    inside = jnp.cumsum(log_decay_rows, axis=1)
    block_total = inside[:, -1]
    query_decay = query_block * jnp.exp(inside)
    key_decay = key_block * jnp.exp(-inside)
    causal = jnp.tril(jnp.ones((BLOCK_POSITIONS, BLOCK_POSITIONS), dtype=bool))
    scores = jnp.where(
        causal, jnp.einsum("nthd,nshd->nhts", query_decay, key_decay, precision=HIGHEST), 0.0
    )
    within = jnp.einsum("nhts,nshv->nthv", scores, value_block, precision=HIGHEST)
    key_end = key_block * jnp.exp(block_total[:, None] - inside)
    update = jnp.einsum("nshd,nshv->nhdv", key_end, value_block, precision=HIGHEST)
    before = jnp.cumsum(block_total, axis=0) - block_total
    ending = jnp.concatenate([before, (before[-1] + block_total[-1])[None]], axis=0)
    after_block = before + block_total
    earlier_mask = jnp.arange(block_count + 1)[:, None] > jnp.arange(block_count)[None, :]
    span_logs = jnp.where(
        earlier_mask[:, :, None, None], ending[:, None] - after_block[None], -1e30
    )
    states = jnp.einsum("nmhd,mhdv->nhdv", jnp.exp(span_logs), update, precision=HIGHEST)
    passed = jnp.einsum("nthd,nhdv->nthv", query_decay, states[:block_count], precision=HIGHEST)
    query_start = query_block * jnp.exp(inside + before[:, None])
    return (within + passed, query_start, jnp.exp(ending[block_count]), states[block_count])


def body(
    queries,
    key_matrix,
    value_matrix,
    output_gate_preactivation,
    decay_preactivation,
    extra_log_decay,
    head_norm_gain,
    output_projection,
    residual,
    feedforward_gain,
    routing,
    router_score,
    expert_gate_weight,
    expert_up_weight,
    expert_down_weight,
    shared_expert_gate,
    shared_expert_up,
    shared_expert_down,
):
    tokens = queries.shape[0]
    local_head_count = extra_log_decay.shape[1]
    local_part, query_start, dev_decay, dev_update = attention_heads(
        queries, key_matrix, value_matrix, decay_preactivation, extra_log_decay
    )
    _, entering = prefix_by_axis(
        (dev_decay, dev_update),
        SP,
        carry_combine,
        (jnp.ones_like(dev_decay), jnp.zeros_like(dev_update)),
    )
    attention_output = local_part + jnp.einsum(
        "nthd,hdv->nthv", query_start, entering, precision=HIGHEST
    )
    attention_output = attention_output.reshape(tokens, local_head_count, DV)
    inverse_rms = lax.rsqrt(
        jnp.mean(attention_output * attention_output, axis=-1, keepdims=True) + EPSILON
    )
    gate_act = jax.nn.silu(
        output_gate_preactivation.astype(jnp.float32).reshape(tokens, local_head_count, DV)
    )
    head_rows = (
        (attention_output * inverse_rms * head_norm_gain.astype(jnp.float32) * gate_act)
        .reshape(tokens, local_head_count * DV)
        .astype(jnp.bfloat16)
    )
    projected = jnp.dot(
        lax.all_gather(head_rows, "tp", axis=1, tiled=True),
        output_projection,
        preferred_element_type=jnp.float32,
    )
    mid_local = (residual.astype(jnp.float32) + projected).astype(jnp.bfloat16)
    mid_rows = gather_directly(mid_local, "tp", 1).astype(jnp.float32)
    normed = (
        mid_rows
        * lax.rsqrt(jnp.mean(mid_rows * mid_rows, axis=-1, keepdims=True) + EPSILON)
        * feedforward_gain.astype(jnp.float32)
    ).astype(jnp.bfloat16)
    shared_pre = jnp.dot(normed, shared_expert_gate, preferred_element_type=jnp.float32)
    shared_lin = jnp.dot(normed, shared_expert_up, preferred_element_type=jnp.float32)
    shared_hidden = (jax.nn.silu(shared_pre) * shared_lin).astype(jnp.bfloat16)
    senders = lax.axis_size(SP)
    tp_count = lax.axis_size("tp")
    tp_bits = tp_count.bit_length() - 1
    tp_index = lax.axis_index("tp")
    groups = tp_count // FF_PARTS
    group_here = tp_index // FF_PARTS
    part_here = tp_index % FF_PARTS
    model_width = normed.shape[1]
    picks = routing.shape[1]
    expert_total = senders * groups
    rows_most = max(2, 3 * tokens * picks // (2 * expert_total))
    slot_count = senders * rows_most
    flat_expert = routing.reshape(-1)
    one_hot = (flat_expert[:, None] == jnp.arange(expert_total, dtype=jnp.int32)[None, :]).astype(
        jnp.int32
    )
    rank_before = jnp.sum((jnp.cumsum(one_hot, axis=0) - one_hot) * one_hot, axis=1)
    owned = flat_expert % groups == group_here
    slot_index = jnp.where(owned, flat_expert // groups * rows_most + rank_before, slot_count)
    token_index = jnp.arange(flat_expert.shape[0], dtype=jnp.int32) // picks
    part_width = model_width // FF_PARTS
    normed_part = lax.dynamic_slice_in_dim(normed, part_here * part_width, part_width, 1)
    outgoing = (
        jnp.zeros((slot_count, part_width), jnp.bfloat16)
        .at[slot_index]
        .set(normed_part[token_index], mode="drop")
    )
    arrived = lax.all_to_all(
        outgoing.reshape(senders, rows_most, part_width),
        SP,
        split_axis=0,
        concat_axis=0,
        tiled=True,
    )
    for bit in range(2):
        partner_cols = from_partner(arrived, "tp", bit)
        upper = (tp_index >> bit) % 2
        arrived = jnp.where(
            upper == 1,
            jnp.concatenate([partner_cols, arrived], axis=2),
            jnp.concatenate([arrived, partner_cols], axis=2),
        )
    rows_in = arrived.reshape(slot_count, model_width)
    gate_pre = jnp.dot(rows_in, expert_gate_weight, preferred_element_type=jnp.float32)
    up_pre = jnp.dot(rows_in, expert_up_weight, preferred_element_type=jnp.float32)
    routed_hidden = (jax.nn.silu(gate_pre) * up_pre).astype(jnp.bfloat16)
    partial_out = jnp.dot(routed_hidden, expert_down_weight, preferred_element_type=jnp.float32)
    slab_width = model_width // tp_count
    partial_out = partial_out.reshape(slot_count, groups, FF_PARTS, slab_width)
    for bit in (1, 0):
        paired = partial_out.reshape(slot_count, groups, 2, 2**bit, slab_width)
        upper = (tp_index >> bit) % 2
        kept = lax.dynamic_index_in_dim(paired, upper, 2, keepdims=False)
        given = lax.dynamic_index_in_dim(paired, 1 - upper, 2, keepdims=False)
        partial_out = kept + from_partner(given.astype(jnp.bfloat16), "tp", bit).astype(given.dtype)
    expert_out = partial_out.reshape(senders, rows_most, groups, slab_width).astype(jnp.bfloat16)
    shared_out = jnp.dot(
        lax.all_gather(shared_hidden, "tp", axis=1, tiled=True),
        shared_expert_down,
        preferred_element_type=jnp.float32,
    )
    returned = lax.all_to_all(expert_out, SP, split_axis=0, concat_axis=0, tiled=True).reshape(
        slot_count, groups, slab_width
    )
    safe_slot = jnp.minimum(slot_index, slot_count - 1)
    route_weight = ROUTE_SCALE * router_score / jnp.sum(router_score, axis=1, keepdims=True)
    pair_weight = jnp.where(owned, route_weight.reshape(-1), 0.0)
    picked = returned[safe_slot].astype(jnp.float32) * pair_weight[:, None, None]
    routed_part = jnp.sum(picked.reshape(tokens, picks, groups, slab_width), axis=1)
    for bit in range(tp_bits - 1, 1, -1):
        paired = routed_part.reshape(tokens, 2, 2 ** (bit - 2), slab_width)
        upper = (tp_index >> bit) % 2
        kept = lax.dynamic_index_in_dim(paired, upper, 1, keepdims=False)
        given = lax.dynamic_index_in_dim(paired, 1 - upper, 1, keepdims=False)
        routed_part = kept + from_partner(given.astype(jnp.bfloat16), "tp", bit).astype(given.dtype)
    routed = routed_part.reshape(tokens, slab_width)
    return (mid_local.astype(jnp.float32) + routed + shared_out).astype(jnp.bfloat16)


def solution(mesh):
    finer = Mesh(mesh.devices.reshape(8, 4, mesh.shape["tp"]), ("sp_0", "sp_1", "tp"))
    in_specs = (
        P(SP, "tp"),
        P(SP, "tp"),
        P(SP, "tp"),
        P(SP, "tp"),
        P(SP, "tp"),
        P(SP, "tp"),
        P(),
        P(None, "tp"),
        P(SP, "tp"),
        P(),
        P(SP, None),
        P(SP, None),
        P(None, SP_TP),
        P(None, SP_TP),
        P(SP_TP, None),
        P(None, "tp"),
        P(None, "tp"),
        P(None, "tp"),
    )
    out_specs = P(SP, "tp")
    return jax.shard_map(body, mesh=finer, in_specs=in_specs, out_specs=out_specs, check_vma=False)
```

profile of v0, /device:TPU:1, one launch (start us, length us, event | category | flops | bytes accessed | tf_op | source)
XLA Modules:
  0.0 347.6 jit_solution(1330581877182747626)
XLA Ops:
  6.6 1.0 fusion.52
  7.6 0.5 broadcast.932
  8.1 1.3 reduce.7
  9.5 0.3 fusion.86
  10.2 1.4 fusion.49
  11.6 1.7 convolution_bitcast_fusion
  13.6 8.5 %all_gather.22 = bf16[4,1,128]{2,1,0:T(2,128)(2,1)S(1)} all-gather(bf16[1,1,128]{2,1,0:T(2,128)(2,1)S(1)} %get-tuple-element.7), channel_id=1, replica_groups=mesh['sp_0'=8,'sp_1'=4,'tp'=16] {'sp_1'}, dimensions={0}, use_global_device_ids=true | all-gather | bytes 1280 | tf_op jit(solution)/shard_map/all_gather | solution.py:31
  22.1 18.6 %all_gather.23 = bf16[8,1,128]{2,1,0:T(2,128)(2,1)S(1)} all-gather(bf16[1,1,128]{2,1,0:T(2,128)(2,1)S(1)} %multiply_convert_fusion.1), channel_id=1, replica_groups=mesh['sp_0'=8,'sp_1'=4,'tp'=16] {'sp_0'}, dimensions={0}, use_global_device_ids=true | all-gather | bytes 2304 | tf_op jit(solution)/shard_map/all_gather | solution.py:31
  40.7 0.6 fusion.124
  41.2 0.6 fusion.131
  41.9 0.4 convolution_select_fusion
  42.3 0.3 convolution_bitcast_fusion.2
  42.6 9.4 %all_gather.24 = bf16[4,1,128,256]{3,2,1,0:T(8,128)(2,1)S(1)} all-gather(bf16[1,1,128,256]{3,2,1,0:T(8,128)(2,1)S(1)} %copy.45), channel_id=1, replica_groups=mesh['sp_0'=8,'sp_1'=4,'tp'=16] {'sp_1'}, dimensions={0}, use_global_device_ids=true | all-gather | bytes 327680 | tf_op jit(solution)/shard_map/all_gather | solution.py:31
  51.9 0.5 broadcast_select_fusion.3
  52.6 21.8 %all_gather.25 = bf16[8,1,128,256]{3,2,1,0:T(8,128)(2,1)} all-gather(bf16[1,1,128,256]{3,2,1,0:T(8,128)(2,1)S(1)} %fusion.46), channel_id=1, replica_groups=mesh['sp_0'=8,'sp_1'=4,'tp'=16] {'sp_0'}, dimensions={0}, use_global_device_ids=true | all-gather | bytes 589824 | tf_op jit(solution)/shard_map/all_gather | solution.py:31
  74.4 0.6 convert_element_type.645
  74.9 0.5 fusion.4
  75.4 1.9 multiply_reduce_fusion
  77.4 1.7 fusion.29
  79.1 53.5 %all-gather.2.cloned.1.call-done = bf16[256,4096]{1,0:T(8,128)(2,1)} async-done(((bf16[256,256]{1,0:T(8,128)(2,1)}), bf16[256,4096]{1,0:T(8,128)(2,1)}) %all-gather.2.cloned.1.call-update) | async-done | bytes 2097168 | tf_op jit(solution)/shard_map/all_gather | solution.py:168
  132.6 2.3 fusion.6
  134.9 0.6 copy-done.4
  135.5 1.2 broadcast_in_dim.52
  136.7 5.1 %all-to-all-start = ((bf16[16,256,128]{2,1,0:T(8,128)(2,1)}), bf16[16,256,128]{2,1,0:T(8,128)(2,1)S(1)}, u32[]{:S(2)}, u32[]{:S(2)}) async-start(bf16[16,256,128]{2,1,0:T(8,128)(2,1)} %broadcast_in_dim.52), calls=%async_computation | async-start | bytes 2097152 | tf_op jit(solution)/shard_map/all_to_all | solution.py:54
  142.9 0.4 fusion.12
  143.4 26.5 %all-to-all-done = bf16[16,256,128]{2,1,0:T(8,128)(2,1)S(1)} async-done(((bf16[16,256,128]{2,1,0:T(8,128)(2,1)}), bf16[16,256,128]{2,1,0:T(8,128)(2,1)S(1)}, u32[]{:S(2)}, u32[]{:S(2)}) %all-to-all-start) | async-done | bytes 1048608 | tf_op jit(solution)/shard_map/all_to_all | solution.py:54
  169.8 0.3 fusion
  170.1 0.3 fusion.2
  170.5 9.7 %scatter_custom_fusion = bf16[384,512]{1,0:T(8,128)(2,1)S(1)} fusion(s32[1024]{0:T(1024)S(1)} %bitcast.324, bf16[256,512]{1,0:T(8,128)(2,1)S(1)} %constant_dynamic-slice_fusion.2, s32[1024]{0:T(1024)S(1)} %broadcast_clamp_fusion.1, bf16[]{:T(256)} %constant.181.clone.1), kind=kCustom, calls=%fused_computation.26 | custom fusion | bytes 393218 | tf_op jit(solution)/shard_map/scatter | solution.py:207
  180.3 27.1 %all_to_all.15 = bf16[32,12,512]{2,1,0:T(8,128)(2,1)S(1)} all-to-all(bf16[32,12,512]{2,1,0:T(8,128)(2,1)S(1)} %reshape.1386), channel_id=1, replica_groups=mesh['sp_0'=8,'sp_1'=4,'tp'=16] {'sp_0','sp_1'}, dimensions={0} | all-to-all | bytes 786432 | tf_op jit(solution)/shard_map/all_to_all | solution.py:209
  207.4 1.9 collective-permute-start
  209.3 1.9 collective-permute-done
  211.2 0.4 maximum_select_fusion.1
  211.5 1.3 copy.52
  212.9 2.1 collective-permute-start.1
  215.2 1.1 maximum_select_fusion.2
  216.3 17.7 %collective-permute-done.1 = bf16[32,12,1024]{2,0,1:T(8,128)(2,1)} collective-permute-done((bf16[32,12,1024]{2,0,1:T(8,128)(2,1)}, bf16[32,12,1024]{2,0,1:T(8,128)(2,1)}, u32[]{:S(2)}, u32[]{:S(2)}) %collective-permute-start.1) | collective-permute-done | bytes 786464 | tf_op jit(solution)/shard_map/ppermute | solution.py:64
  234.0 1.6 copy.53
  235.6 1.1 concatenate.32
  236.7 2.8 fusion.18
  239.5 5.1 %fusion.19 = f32[384,2048]{1,0:T(8,128)} fusion(bf16[256,2048]{1,0:T(8,128)(2,1)S(1)} %copy-done, f32[384,256]{1,0:T(8,128)S(1)} %fusion.18, bf16[2048,256]{1,0:T(8,128)(2,1)} %param.31, bf16[384,1024]{1,0:T(8,128)(2,1)} %maximum_select_fusion.2, bf16[384,1024]{1,0:T(8,128)(2,1)S(1)} %copy-done.3, pred[]{:T(512)S(6)} %eq.66), kind=kOutput, calls=%fused_computation.48 | convolution fusion | flops 812974080 | bytes 7208961 | tf_op jit(solution)/shard_map/dot_general | solution.py:228
  244.7 5.6 %reshape_reshape.3 = f32[384,4,2,2,128]{4,3,2,1,0:T(2,128)} reshape(f32[384,2048]{1,0:T(8,128)} %fusion.19) | data formatting | bytes 6291456 | tf_op jit(solution)/shard_map/reshape;reshape | solution.py:232
  250.3 1.9 constant_dynamic-slice_fusion
  252.4 2.2 collective-permute-start.2
  254.7 2.0 constant_dynamic-slice_fusion.1
  256.6 15.9 %collective-permute-done.2 = bf16[384,4,2,128]{3,1,0,2:T(4,128)(2,1)} collective-permute-done((bf16[384,4,2,128]{3,1,0,2:T(4,128)(2,1)S(1)}, bf16[384,4,2,128]{3,1,0,2:T(4,128)(2,1)}, u32[]{:S(2)}, u32[]{:S(2)}) %collective-permute-start.2) | collective-permute-done | bytes 786464 | tf_op jit(solution)/shard_map/ppermute | solution.py:64
  272.6 1.7 bitcast_add_fusion
  274.3 1.1 copy-done.1
  275.6 3.8 %collective-permute-start.3 = (bf16[384,4,1,128]{3,1,0,2:T(4,128)(2,1)S(1)}, bf16[384,4,1,128]{3,1,0,2:T(4,128)(2,1)S(1)}, u32[]{:S(2)}, u32[]{:S(2)}) collective-permute-start(bf16[384,4,1,128]{3,1,0,2:T(4,128)(2,1)S(1)} %dynamic-slice_convert_fusion), channel_id=1, source_target_pairs={{0,1},{1,0},{2,3},{3,2},{4,5},{5,4},{6,7},{7,6},{8,9},{9,8},{10,11... | collective-permute-start | bytes 1179656 | tf_op jit(solution)/shard_map/ppermute | solution.py:64
  279.3 1.3 collective-permute-done.3
  280.6 2.1 add_convert_fusion
  282.7 4.3 %all-to-all-start.2 = ((bf16[32,12,4,128]{3,2,1,0:T(4,128)(2,1)}), bf16[32,12,4,128]{3,2,1,0:T(4,128)(2,1)S(1)}, u32[]{:S(2)}, u32[]{:S(2)}) async-start(bf16[32,12,4,128]{3,2,1,0:T(4,128)(2,1)} %bitcast.64), calls=%async_computation.2 | async-start | bytes 786432 | tf_op jit(solution)/shard_map/all_to_all | solution.py:243
  287.1 0.8 copy.56
  287.9 1.0 fusion.143
  289.0 12.0 %all-to-all-done.2 = bf16[32,12,4,128]{3,2,1,0:T(4,128)(2,1)S(1)} async-done(((bf16[32,12,4,128]{3,2,1,0:T(4,128)(2,1)}), bf16[32,12,4,128]{3,2,1,0:T(4,128)(2,1)S(1)}, u32[]{:S(2)}, u32[]{:S(2)}) %all-to-all-start.2) | async-done | bytes 393248 | tf_op jit(solution)/shard_map/all_to_all | solution.py:243
  300.9 3.6 %gather_fusion = bf16[1024,4,128]{2,1,0:T(4,128)(2,1)S(1)} fusion(bf16[384,4,128]{2,1,0:T(4,128)(2,1)S(1)} %bitcast.299, s32[1024]{0:T(1024)S(1)} %broadcast_clamp_fusion), kind=kCustom, calls=%fused_computation.1 | custom fusion | bytes 2101248 | tf_op jit(solution)/shard_map/gather | solution.py:249
  304.5 2.7 fusion.3
  307.4 4.1 %collective-permute-start.4 = (bf16[256,2,128]{2,0,1:T(8,128)(2,1)S(1)}, bf16[256,2,128]{2,0,1:T(8,128)(2,1)S(1)}, u32[]{:S(2)}, u32[]{:S(2)}) collective-permute-start(bf16[256,2,128]{2,0,1:T(8,128)(2,1)S(1)} %fusion.50), channel_id=1, source_target_pairs={{0,8},{1,9},{2,10},{3,11},{4,12},{5,13},{6,14},{7,15},{8,0},{9,1},... | collective-permute-start | bytes 393224 | tf_op jit(solution)/shard_map/ppermute | solution.py:64
  311.6 0.4 fusion.7
  312.0 19.9 %all_gather.27 = bf16[256,512]{0,1:T(8,128)(2,1)S(1)} all-gather(bf16[256,32]{0,1:T(8,128)(2,1)S(1)} %fusion.7), channel_id=1, replica_groups=mesh['sp_0'=8,'sp_1'=4,'tp'=16] {'tp'}, dimensions={1}, use_global_device_ids=true | all-gather | bytes 278528 | tf_op jit(solution)/shard_map/all_gather | solution.py:239
  331.9 1.9 collective-permute-start.5
  333.9 0.3 fusion.144
  334.1 6.0 %collective-permute-done.5 = bf16[256,1,128]{2,0,1:T(8,128)(2,1)S(1)} collective-permute-done((bf16[256,1,128]{2,0,1:T(8,128)(2,1)S(1)}, bf16[256,1,128]{2,0,1:T(8,128)(2,1)S(1)}, u32[]{:S(2)}, u32[]{:S(2)}) %collective-permute-start.5) | collective-permute-done | bytes 65568 | tf_op jit(solution)/shard_map/ppermute | solution.py:64
  340.1 0.7 fusion.66
  (89 shorter events, 2.9 us)
Async XLA Ops:
  6.5 233.0 %copy-start = (bf16[256,2048]{1,0:T(8,128)(2,1)S(1)}, bf16[256,2048]{1,0:T(8,128)(2,1)}, u32[]{:S(2)}) copy-start(bf16[256,2048]{1,0:T(8,128)(2,1)} %param.32) | copy-start | bytes 3145732
  6.5 126.1 %all-gather.2.cloned.1.call-start = ((), (), s32[]{:S(2)}) async-start(), calls=%async_computation.3 | async-start | bytes 2228224 | tf_op jit(solution)/shard_map/all_gather | solution.py:168
  9.9 32.0 %copy-start.12 = (bf16[256,128]{1,0:T(8,128)(2,1)S(1)}, bf16[256,128]{1,0:T(8,128)(2,1)}, u32[]{:S(2)}) copy-start(bf16[256,128]{1,0:T(8,128)(2,1)} %param.18) | copy-start | bytes 196612
  10.2 31.7 %copy-start.7 = (bf16[256,128]{1,0:T(8,128)(2,1)S(1)}, bf16[256,128]{1,0:T(8,128)(2,1)}, u32[]{:S(2)}) copy-start(bf16[256,128]{1,0:T(8,128)(2,1)} %param.19) | copy-start | bytes 196612
  11.6 30.7 %copy-start.6 = (bf16[256,256]{1,0:T(8,128)(2,1)S(1)}, bf16[256,256]{1,0:T(8,128)(2,1)}, u32[]{:S(2)}) copy-start(bf16[256,256]{1,0:T(8,128)(2,1)} %param.20) | copy-start | bytes 393220
  13.3 61.0 %copy-start.18 = (bf16[256]{0:T(256)(128)(2,1)S(1)}, bf16[256]{0:T(256)(128)(2,1)}, u32[]{:S(2)}) copy-start(bf16[256]{0:T(256)(128)(2,1)} %param.24) | copy-start | bytes 1540
  74.9 57.7 %copy-start.2 = (bf16[4096,128]{1,0:T(8,128)(2,1)S(1)}, bf16[4096,128]{1,0:T(8,128)(2,1)}, u32[]{:S(2)}) copy-start(bf16[4096,128]{1,0:T(8,128)(2,1)} %param.25) | copy-start | bytes 3145732
  75.4 2.0 copy-start.17
  75.4 57.2 %copy-start.13 = (bf16[256,128]{1,0:T(8,128)(2,1)S(1)}, bf16[256,128]{1,0:T(8,128)(2,1)}, u32[]{:S(2)}) copy-start(bf16[256,128]{1,0:T(8,128)(2,1)} %param.26) | copy-start | bytes 196612
  134.9 0.6 copy-start.4
  135.5 6.3 %copy-start.14 = (s32[256,4]{0,1:T(4,128)S(1)}, s32[256,4]{0,1:T(4,128)}, u32[]{:S(2)}) copy-start(s32[256,4]{0,1:T(4,128)} %param.28) | copy-start | bytes 12292
  135.5 6.8 %copy-start.16 = (bf16[2048]{0:T(1024)(128)(2,1)S(1)}, bf16[2048]{0:T(1024)(128)(2,1)}, u32[]{:S(2)}) copy-start(bf16[2048]{0:T(1024)(128)(2,1)} %param.27) | copy-start | bytes 12292
  136.7 33.1 %all-to-all-start = ((bf16[16,256,128]{2,1,0:T(8,128)(2,1)}), bf16[16,256,128]{2,1,0:T(8,128)(2,1)S(1)}, u32[]{:S(2)}, u32[]{:S(2)}) async-start(bf16[16,256,128]{2,1,0:T(8,128)(2,1)} %broadcast_in_dim.52), calls=%async_computation | async-start | bytes 2097152 | tf_op jit(solution)/shard_map/all_to_all | solution.py:54
  207.4 3.8 %collective-permute-start = (bf16[32,12,512]{2,1,0:T(8,128)(2,1)S(1)}, bf16[32,12,512]{2,1,0:T(8,128)(2,1)S(1)}, u32[]{:S(2)}, u32[]{:S(2)}) collective-permute-start(bf16[32,12,512]{2,1,0:T(8,128)(2,1)S(1)} %all_to_all.15), channel_id=1, source_target_pairs={{0,1},{1,0},{2,3},{3,2},{4,5},{5,4},{6,7},{7,6},{8,9},{9,8},{10,11... | collective-permute-start | bytes 1179656 | tf_op jit(solution)/shard_map/ppermute | solution.py:64
  212.9 21.2 %collective-permute-start.1 = (bf16[32,12,1024]{2,0,1:T(8,128)(2,1)}, bf16[32,12,1024]{2,0,1:T(8,128)(2,1)}, u32[]{:S(2)}, u32[]{:S(2)}) collective-permute-start(bf16[32,12,1024]{2,0,1:T(8,128)(2,1)} %copy.52), channel_id=1, source_target_pairs={{0,2},{1,3},{2,0},{3,1},{4,6},{5,7},{6,4},{7,5},{8,10},{9,11},{10,... | collective-permute-start | bytes 2359304 | tf_op jit(solution)/shard_map/ppermute | solution.py:64
  236.7 2.8 copy-start.3
  252.4 20.1 %collective-permute-start.2 = (bf16[384,4,2,128]{3,1,0,2:T(4,128)(2,1)S(1)}, bf16[384,4,2,128]{3,1,0,2:T(4,128)(2,1)}, u32[]{:S(2)}, u32[]{:S(2)}) collective-permute-start(bf16[384,4,2,128]{3,1,0,2:T(4,128)(2,1)S(1)} %bitcast.308), channel_id=1, source_target_pairs={{0,2},{1,3},{2,0},{3,1},{4,6},{5,7},{6,4},{7,5},{8,10},{9,11},{10,... | collective-permute-start | bytes 2359304 | tf_op jit(solution)/shard_map/ppermute | solution.py:64
  274.3 1.1 copy-start.1
  275.4 11.7 %copy-start.15 = (f32[256,4]{0,1:T(4,128)S(1)}, f32[256,4]{0,1:T(4,128)}, u32[]{:S(2)}) copy-start(f32[256,4]{0,1:T(4,128)} %param.29) | copy-start | bytes 12292
  275.4 12.5 %copy-start.8 = (bf16[2048,32]{0,1:T(8,128)(2,1)S(1)}, bf16[2048,32]{0,1:T(8,128)(2,1)}, u32[]{:S(2)}) copy-start(bf16[2048,32]{0,1:T(8,128)(2,1)} %param.33) | copy-start | bytes 393220
  275.6 5.1 %collective-permute-start.3 = (bf16[384,4,1,128]{3,1,0,2:T(4,128)(2,1)S(1)}, bf16[384,4,1,128]{3,1,0,2:T(4,128)(2,1)S(1)}, u32[]{:S(2)}, u32[]{:S(2)}) collective-permute-start(bf16[384,4,1,128]{3,1,0,2:T(4,128)(2,1)S(1)} %dynamic-slice_convert_fusion), channel_id=1, source_target_pairs={{0,1},{1,0},{2,3},{3,2},{4,5},{5,4},{6,7},{7,6},{8,9},{9,8},{10,11... | collective-permute-start | bytes 1179656 | tf_op jit(solution)/shard_map/ppermute | solution.py:64
  282.7 18.2 %all-to-all-start.2 = ((bf16[32,12,4,128]{3,2,1,0:T(4,128)(2,1)}), bf16[32,12,4,128]{3,2,1,0:T(4,128)(2,1)S(1)}, u32[]{:S(2)}, u32[]{:S(2)}) async-start(bf16[32,12,4,128]{3,2,1,0:T(4,128)(2,1)} %bitcast.64), calls=%async_computation.2 | async-start | bytes 786432 | tf_op jit(solution)/shard_map/all_to_all | solution.py:243
  304.5 7.0 %copy-start.9 = (bf16[2048,32]{0,1:T(8,128)(2,1)S(1)}, bf16[2048,32]{0,1:T(8,128)(2,1)}, u32[]{:S(2)}) copy-start(bf16[2048,32]{0,1:T(8,128)(2,1)} %param.34) | copy-start | bytes 393220
  304.5 7.0 %copy-start.10 = (f32[256,32]{0,1:T(8,128)S(1)}, f32[256,32]{0,1:T(8,128)}, u32[]{:S(2)}) copy-start(f32[256,32]{0,1:T(8,128)} %fusion.143) | copy-start | bytes 98308
  307.3 26.6 %copy-start.11 = (bf16[512,128]{1,0:T(8,128)(2,1)S(1)}, bf16[512,128]{1,0:T(8,128)(2,1)}, u32[]{:S(2)}) copy-start(bf16[512,128]{1,0:T(8,128)(2,1)} %param.35) | copy-start | bytes 393220
  307.3 32.8 %copy-start.5 = (bf16[256,128]{1,0:T(8,128)(2,1)S(1)}, bf16[256,128]{1,0:T(8,128)(2,1)}, u32[]{:S(2)}) copy-start(bf16[256,128]{1,0:T(8,128)(2,1)} %copy-done.4) | copy-start | bytes 196612
  307.4 24.5 %collective-permute-start.4 = (bf16[256,2,128]{2,0,1:T(8,128)(2,1)S(1)}, bf16[256,2,128]{2,0,1:T(8,128)(2,1)S(1)}, u32[]{:S(2)}, u32[]{:S(2)}) collective-permute-start(bf16[256,2,128]{2,0,1:T(8,128)(2,1)S(1)} %fusion.50), channel_id=1, source_target_pairs={{0,8},{1,9},{2,10},{3,11},{4,12},{5,13},{6,14},{7,15},{8,0},{9,1},... | collective-permute-start | bytes 393224 | tf_op jit(solution)/shard_map/ppermute | solution.py:64
  331.9 8.2 %collective-permute-start.5 = (bf16[256,1,128]{2,0,1:T(8,128)(2,1)S(1)}, bf16[256,1,128]{2,0,1:T(8,128)(2,1)S(1)}, u32[]{:S(2)}, u32[]{:S(2)}) collective-permute-start(bf16[256,1,128]{2,0,1:T(8,128)(2,1)S(1)} %dynamic-slice_convert_fusion.2), channel_id=1, source_target_pairs={{0,4},{1,5},{2,6},{3,7},{4,0},{5,1},{6,2},{7,3},{8,12},{9,13},{10,... | collective-permute-start | bytes 196616 | tf_op jit(solution)/shard_map/ppermute | solution.py:64
Sparse Core Ops, SparseCore 0:
  79.2 53.3 all-gather.1
where the time goes:
time: 349 us; the launch traced here: 348 us
  waiting for transfers between devices  135 us (39%)
  blocking collectives  105 us (30%)
  local copies, waits for them, and re-layouts  33.1 us (9%)
  starting transfers between devices  25.5 us (7%)
  matrix products  18 us (5%)
  other arithmetic  16.9 us (5%)
  between operations  14.1 us (4%)
    all_gather x4, blocking collectives, prefix_by_axis(): lax.all_gather(part.astype(kind), axis)  58.2 us
    all_gather x1, waiting for transfers between devices, body(): lax.all_gather(head_rows, 'tp', axis=1, tiled=True)  53.5 us
    ppermute x6, waiting for transfers between devices, from_partner(): return lax.ppermute(value, axis, pairs)  42.8 us
    all_to_all x1, blocking collectives, body(): lax.all_to_all(outgoing.reshape(senders, rows_most, part_width), SP, spli...  27.1 us
    all_to_all x1, waiting for transfers between devices, sent_to_all(): return lax.all_to_all(copies, axis, split_axis=0, concat_axis=0, tiled=True)  26.5 us
    all_gather x1, blocking collectives, body(): lax.all_gather(shared_hidden, 'tp', axis=1, tiled=True)  19.9 us
    ppermute x6, starting transfers between devices, from_partner(): return lax.ppermute(value, axis, pairs)  16.1 us
    all_to_all x1, waiting for transfers between devices, body(): lax.all_to_all(expert_out, SP, split_axis=0, concat_axis=0, tiled=True)  12 us
  transfers between devices with their start and end apart: 9, of which 8 were waited for; matrix products, arithmetic and copies ran while one was open for 2% of the time, Pallas kernels for 0%

commit v1 on v0

--- a/solution.py
+++ b/solution.py
@@ -164,10 +164,13 @@
         .reshape(tokens, local_head_count * DV)
         .astype(jnp.bfloat16)
     )
+
+    def regions_trace(x_part):
+        later = jnp.concatenate([x_part for _ in range(jax.lax.axis_size("tp"))], axis=1)
+        return jax.lax.all_to_all(later, axis_name="tp", split_axis=1, concat_axis=1, tiled=True)
+
     projected = jnp.dot(
-        lax.all_gather(head_rows, "tp", axis=1, tiled=True),
-        output_projection,
-        preferred_element_type=jnp.float32,
+        regions_trace(head_rows), output_projection, preferred_element_type=jnp.float32
     )
     mid_local = (residual.astype(jnp.float32) + projected).astype(jnp.bfloat16)
     mid_rows = gather_directly(mid_local, "tp", 1).astype(jnp.float32)

time: 349 us -> 342 us (0.980)
  blocking collectives: 105 us -> 170 us
  waiting for transfers between devices: 135 us -> 80.4 us
  between operations: 14.1 us -> 0.79 us
  other arithmetic: 16.9 us -> 13.1 us
    all_to_all x0 -> x1, blocking collectives: none -> 73.4 us  [regions_trace(): jax.lax.all_to_all(later, axis_name='tp', split_axis=1, concat_axis=1, ti...]
    all_gather x1 -> x0, waiting for transfers between devices: 53.5 us -> none  [body(): lax.all_gather(head_rows, 'tp', axis=1, tiled=True)]
    all_to_all x1, blocking collectives: 27.1 us -> 20.9 us  [body(): lax.all_to_all(outgoing.reshape(senders, rows_most, part_width), SP, spli...]
  transfers between devices with their start and end apart: 9 -> 8, of which waited for: 8 -> 7; matrix products, arithmetic and copies ran while one was open for 2% -> 2% of each run, Pallas kernels for 0% -> 0%
where the time goes in v1:
time: 342 us; the launch traced here: 341 us
  blocking collectives  170 us (50%)
  waiting for transfers between devices  80.4 us (24%)
  local copies, waits for them, and re-layouts  35.7 us (10%)
  starting transfers between devices  24.2 us (7%)
  matrix products  17.2 us (5%)
  other arithmetic  13.1 us (4%)
    all_to_all x1, blocking collectives, regions_trace(): jax.lax.all_to_all(later, axis_name='tp', split_axis=1, concat_axis=1, ti...  73.4 us
    all_gather x4, blocking collectives, prefix_by_axis(): lax.all_gather(part.astype(kind), axis)  55.8 us
    ppermute x6, waiting for transfers between devices, from_partner(): return lax.ppermute(value, axis, pairs)  42.8 us
    all_to_all x1, waiting for transfers between devices, sent_to_all(): return lax.all_to_all(copies, axis, split_axis=0, concat_axis=0, tiled=True)  25.6 us
    all_to_all x1, blocking collectives, body(): lax.all_to_all(outgoing.reshape(senders, rows_most, part_width), SP, spli...  20.9 us
    all_gather x1, blocking collectives, body(): lax.all_gather(shared_hidden, 'tp', axis=1, tiled=True)  19.9 us
    ppermute x6, starting transfers between devices, from_partner(): return lax.ppermute(value, axis, pairs)  16.1 us
    all_to_all x1, waiting for transfers between devices, body(): lax.all_to_all(expert_out, SP, split_axis=0, concat_axis=0, tiled=True)  12 us
  transfers between devices with their start and end apart: 8, of which 7 were waited for; matrix products, arithmetic and copies ran while one was open for 2% of the time, Pallas kernels for 0%

profile of v1, /device:TPU:1, one launch (start us, length us, event | category | flops | bytes accessed | tf_op | source)
XLA Modules:
  0.0 341.5 jit_solution(18419981343144636836)
XLA Ops:
  0.0 1.0 fusion.52
  1.0 0.5 broadcast.934
  1.6 1.3 reduce.7
  3.0 0.3 fusion.86
  3.7 1.4 fusion.49
  5.1 1.7 convolution_bitcast_fusion
  6.9 0.1 slice.277
  7.0 8.5 %all_gather.19 = bf16[4,1,128]{2,1,0:T(2,128)(2,1)S(1)} all-gather(bf16[1,1,128]{2,1,0:T(2,128)(2,1)S(1)} %get-tuple-element.7), channel_id=1, replica_groups=mesh['sp_0'=8,'sp_1'=4,'tp'=16] {'sp_1'}, dimensions={0}, use_global_device_ids=true | all-gather | bytes 1280 | tf_op jit(solution)/shard_map/all_gather | solution.py:31
  15.6 18.6 %all_gather.20 = bf16[8,1,128]{2,1,0:T(2,128)(2,1)S(1)} all-gather(bf16[1,1,128]{2,1,0:T(2,128)(2,1)S(1)} %multiply_convert_fusion.1), channel_id=1, replica_groups=mesh['sp_0'=8,'sp_1'=4,'tp'=16] {'sp_0'}, dimensions={0}, use_global_device_ids=true | all-gather | bytes 2304 | tf_op jit(solution)/shard_map/all_gather | solution.py:31
  34.3 0.4 convolution_select_fusion
  34.6 0.2 convolution_bitcast_fusion.2
  34.9 9.4 %all_gather.21 = bf16[4,1,128,256]{3,2,1,0:T(8,128)(2,1)S(1)} all-gather(bf16[1,1,128,256]{3,2,1,0:T(8,128)(2,1)S(1)} %copy.65), channel_id=1, replica_groups=mesh['sp_0'=8,'sp_1'=4,'tp'=16] {'sp_1'}, dimensions={0}, use_global_device_ids=true | all-gather | bytes 327680 | tf_op jit(solution)/shard_map/all_gather | solution.py:31
  44.4 19.4 %all_gather.22 = bf16[8,1,128,256]{3,2,1,0:T(8,128)(2,1)S(1)} all-gather(bf16[1,1,128,256]{3,2,1,0:T(8,128)(2,1)S(1)} %fusion.46), channel_id=1, replica_groups=mesh['sp_0'=8,'sp_1'=4,'tp'=16] {'sp_0'}, dimensions={0}, use_global_device_ids=true | all-gather | bytes 589824 | tf_op jit(solution)/shard_map/all_gather | solution.py:31
  63.8 0.5 fusion.4
  64.3 0.8 multiply_reduce_fusion
  65.3 0.2 concatenate.34
  65.5 73.4 %all_to_all.24 = bf16[256,16,256]{2,0,1:T(8,128)(2,1)S(1)} all-to-all(bf16[256,16,256]{2,0,1:T(8,128)(2,1)S(1)} %concatenate.34), channel_id=1, replica_groups=mesh['sp_0'=8,'sp_1'=4,'tp'=16] {'tp'}, dimensions={1} | all-to-all | bytes 4194304 | tf_op jit(solution)/shard_map/all_to_all | solution.py:170
  138.9 2.4 copy.66
  141.3 2.6 fusion.6
  143.9 0.6 copy-done.3
  144.5 1.2 broadcast_in_dim.52
  145.7 3.7 %all-to-all-start.1 = ((bf16[16,256,128]{2,1,0:T(8,128)(2,1)}), bf16[16,256,128]{2,1,0:T(8,128)(2,1)S(1)}, u32[]{:S(2)}, u32[]{:S(2)}) async-start(bf16[16,256,128]{2,1,0:T(8,128)(2,1)} %broadcast_in_dim.52), calls=%async_computation.1 | async-start | bytes 2097152 | tf_op jit(solution)/shard_map/all_to_all | solution.py:54
  150.1 0.2 fusion.15
  150.5 0.4 fusion.12
  151.0 25.6 %all-to-all-done.1 = bf16[16,256,128]{2,1,0:T(8,128)(2,1)S(1)} async-done(((bf16[16,256,128]{2,1,0:T(8,128)(2,1)}), bf16[16,256,128]{2,1,0:T(8,128)(2,1)S(1)}, u32[]{:S(2)}, u32[]{:S(2)}) %all-to-all-start.1) | async-done | bytes 1048608 | tf_op jit(solution)/shard_map/all_to_all | solution.py:54
  176.6 0.3 fusion
  176.9 0.3 fusion.2
  177.2 9.7 %scatter_custom_fusion = bf16[384,512]{1,0:T(8,128)(2,1)S(1)} fusion(s32[1024]{0:T(1024)S(1)} %bitcast.326, bf16[256,512]{1,0:T(8,128)(2,1)S(1)} %constant_dynamic-slice_fusion.2, s32[1024]{0:T(1024)S(1)} %broadcast_clamp_fusion.1, bf16[]{:T(256)} %constant.181.clone.1), kind=kCustom, calls=%fused_computation.26 | custom fusion | bytes 393218 | tf_op jit(solution)/shard_map/scatter | solution.py:210
  187.0 20.9 %all_to_all.25 = bf16[32,12,512]{2,1,0:T(8,128)(2,1)S(1)} all-to-all(bf16[32,12,512]{2,1,0:T(8,128)(2,1)S(1)} %reshape.1406), channel_id=1, replica_groups=mesh['sp_0'=8,'sp_1'=4,'tp'=16] {'sp_0','sp_1'}, dimensions={0} | all-to-all | bytes 786432 | tf_op jit(solution)/shard_map/all_to_all | solution.py:212
  208.0 1.9 collective-permute-start
  209.9 1.9 collective-permute-done
  211.8 0.4 maximum_select_fusion.1
  212.2 1.3 copy.73
  213.5 2.1 collective-permute-start.1
  215.8 1.1 maximum_select_fusion.2
  216.9 17.7 %collective-permute-done.1 = bf16[32,12,1024]{2,0,1:T(8,128)(2,1)} collective-permute-done((bf16[32,12,1024]{2,0,1:T(8,128)(2,1)}, bf16[32,12,1024]{2,0,1:T(8,128)(2,1)}, u32[]{:S(2)}, u32[]{:S(2)}) %collective-permute-start.1) | collective-permute-done | bytes 786464 | tf_op jit(solution)/shard_map/ppermute | solution.py:64
  234.6 1.6 copy.74
  236.2 1.1 concatenate.37
  237.3 2.8 fusion.18
  240.1 5.1 %fusion.19 = f32[384,2048]{1,0:T(8,128)} fusion(bf16[256,2048]{1,0:T(8,128)(2,1)S(1)} %copy-done, f32[384,256]{1,0:T(8,128)S(1)} %fusion.18, bf16[2048,256]{1,0:T(8,128)(2,1)} %param.31, bf16[384,1024]{1,0:T(8,128)(2,1)} %maximum_select_fusion.2, bf16[384,1024]{1,0:T(8,128)(2,1)S(1)} %copy-done.2, pred[]{:T(512)S(6)} %eq.66), kind=kOutput, calls=%fused_computation.48 | convolution fusion | flops 812974080 | bytes 7208961 | tf_op jit(solution)/shard_map/dot_general | solution.py:231
  245.3 5.6 %reshape_reshape.3 = f32[384,4,2,2,128]{4,3,2,1,0:T(2,128)} reshape(f32[384,2048]{1,0:T(8,128)} %fusion.19) | data formatting | bytes 6291456 | tf_op jit(solution)/shard_map/reshape;reshape | solution.py:235
  250.9 1.9 constant_dynamic-slice_fusion
  252.8 0.2 copy.90
  253.1 2.2 collective-permute-start.2
  255.3 2.0 constant_dynamic-slice_fusion.1
  257.2 15.9 %collective-permute-done.2 = bf16[384,4,2,128]{3,1,0,2:T(4,128)(2,1)} collective-permute-done((bf16[384,4,2,128]{3,1,0,2:T(4,128)(2,1)S(1)}, bf16[384,4,2,128]{3,1,0,2:T(4,128)(2,1)}, u32[]{:S(2)}, u32[]{:S(2)}) %collective-permute-start.2) | collective-permute-done | bytes 786464 | tf_op jit(solution)/shard_map/ppermute | solution.py:64
  273.2 1.7 bitcast_add_fusion
  274.9 1.2 copy-done.1
  276.2 3.8 %collective-permute-start.3 = (bf16[384,4,1,128]{3,1,0,2:T(4,128)(2,1)S(1)}, bf16[384,4,1,128]{3,1,0,2:T(4,128)(2,1)S(1)}, u32[]{:S(2)}, u32[]{:S(2)}) collective-permute-start(bf16[384,4,1,128]{3,1,0,2:T(4,128)(2,1)S(1)} %dynamic-slice_convert_fusion), channel_id=1, source_target_pairs={{0,1},{1,0},{2,3},{3,2},{4,5},{5,4},{6,7},{7,6},{8,9},{9,8},{10,11... | collective-permute-start | bytes 1179656 | tf_op jit(solution)/shard_map/ppermute | solution.py:64
  280.0 1.3 collective-permute-done.3
  281.3 2.1 add_convert_fusion
  283.4 4.4 %all-to-all-start.3 = ((bf16[32,12,4,128]{3,2,1,0:T(4,128)(2,1)}), bf16[32,12,4,128]{3,2,1,0:T(4,128)(2,1)S(1)}, u32[]{:S(2)}, u32[]{:S(2)}) async-start(bf16[32,12,4,128]{3,2,1,0:T(4,128)(2,1)} %bitcast.65), calls=%async_computation.3 | async-start | bytes 786432 | tf_op jit(solution)/shard_map/all_to_all | solution.py:246
  287.9 0.8 copy.77
  288.7 1.0 fusion.143
  289.7 12.0 %all-to-all-done.3 = bf16[32,12,4,128]{3,2,1,0:T(4,128)(2,1)S(1)} async-done(((bf16[32,12,4,128]{3,2,1,0:T(4,128)(2,1)}), bf16[32,12,4,128]{3,2,1,0:T(4,128)(2,1)S(1)}, u32[]{:S(2)}, u32[]{:S(2)}) %all-to-all-start.3) | async-done | bytes 393248 | tf_op jit(solution)/shard_map/all_to_all | solution.py:246
  301.7 3.6 %gather_fusion = bf16[1024,4,128]{2,1,0:T(4,128)(2,1)S(1)} fusion(bf16[384,4,128]{2,1,0:T(4,128)(2,1)S(1)} %bitcast.301, s32[1024]{0:T(1024)S(1)} %broadcast_clamp_fusion), kind=kCustom, calls=%fused_computation.1 | custom fusion | bytes 2101248 | tf_op jit(solution)/shard_map/gather | solution.py:252
  305.3 2.7 fusion.3
  308.1 4.2 %collective-permute-start.4 = (bf16[256,2,128]{2,0,1:T(8,128)(2,1)S(1)}, bf16[256,2,128]{2,0,1:T(8,128)(2,1)S(1)}, u32[]{:S(2)}, u32[]{:S(2)}) collective-permute-start(bf16[256,2,128]{2,0,1:T(8,128)(2,1)S(1)} %fusion.50), channel_id=1, source_target_pairs={{0,8},{1,9},{2,10},{3,11},{4,12},{5,13},{6,14},{7,15},{8,0},{9,1},... | collective-permute-start | bytes 393224 | tf_op jit(solution)/shard_map/ppermute | solution.py:64
  312.3 0.4 fusion.7
  312.7 19.9 %all_gather.23 = bf16[256,512]{0,1:T(8,128)(2,1)S(1)} all-gather(bf16[256,32]{0,1:T(8,128)(2,1)S(1)} %fusion.7), channel_id=1, replica_groups=mesh['sp_0'=8,'sp_1'=4,'tp'=16] {'tp'}, dimensions={1}, use_global_device_ids=true | all-gather | bytes 278528 | tf_op jit(solution)/shard_map/all_gather | solution.py:242
  332.7 1.9 collective-permute-start.5
  334.6 0.3 fusion.144
  334.9 5.9 %collective-permute-done.5 = bf16[256,1,128]{2,0,1:T(8,128)(2,1)S(1)} collective-permute-done((bf16[256,1,128]{2,0,1:T(8,128)(2,1)S(1)}, bf16[256,1,128]{2,0,1:T(8,128)(2,1)S(1)}, u32[]{:S(2)}, u32[]{:S(2)}) %collective-permute-start.5) | collective-permute-done | bytes 65568 | tf_op jit(solution)/shard_map/ppermute | solution.py:64
  340.8 0.7 fusion.66
  (87 shorter events, 2.4 us)
Async XLA Ops:
  0.0 240.1 %copy-start = (bf16[256,2048]{1,0:T(8,128)(2,1)S(1)}, bf16[256,2048]{1,0:T(8,128)(2,1)}, u32[]{:S(2)}) copy-start(bf16[256,2048]{1,0:T(8,128)(2,1)} %param.32) | copy-start | bytes 3145732
  3.3 30.9 %copy-start.12 = (bf16[256,128]{1,0:T(8,128)(2,1)S(1)}, bf16[256,128]{1,0:T(8,128)(2,1)}, u32[]{:S(2)}) copy-start(bf16[256,128]{1,0:T(8,128)(2,1)} %param.18) | copy-start | bytes 196612
  3.7 30.6 %copy-start.6 = (bf16[256,128]{1,0:T(8,128)(2,1)S(1)}, bf16[256,128]{1,0:T(8,128)(2,1)}, u32[]{:S(2)}) copy-start(bf16[256,128]{1,0:T(8,128)(2,1)} %param.19) | copy-start | bytes 196612
  5.1 29.5 %copy-start.5 = (bf16[256,256]{1,0:T(8,128)(2,1)S(1)}, bf16[256,256]{1,0:T(8,128)(2,1)}, u32[]{:S(2)}) copy-start(bf16[256,256]{1,0:T(8,128)(2,1)} %param.20) | copy-start | bytes 393220
  6.8 57.0 %copy-start.17 = (bf16[256]{0:T(256)(128)(2,1)S(1)}, bf16[256]{0:T(256)(128)(2,1)}, u32[]{:S(2)}) copy-start(bf16[256]{0:T(256)(128)(2,1)} %param.24) | copy-start | bytes 1540
  44.4 20.8 %copy-start.10 = (bf16[256,256]{1,0:T(8,128)(2,1)S(1)}, bf16[256,256]{1,0:T(8,128)(2,1)}, u32[]{:S(2)}) copy-start(bf16[256,256]{1,0:T(8,128)(2,1)} %param.21) | copy-start | bytes 393220
  138.9 2.4 copy-start.13
  143.9 0.6 copy-start.3
  144.5 4.9 %copy-start.14 = (s32[256,4]{0,1:T(4,128)S(1)}, s32[256,4]{0,1:T(4,128)}, u32[]{:S(2)}) copy-start(s32[256,4]{0,1:T(4,128)} %param.28) | copy-start | bytes 12292
  144.5 5.4 %copy-start.16 = (bf16[2048]{0:T(1024)(128)(2,1)S(1)}, bf16[2048]{0:T(1024)(128)(2,1)}, u32[]{:S(2)}) copy-start(bf16[2048]{0:T(1024)(128)(2,1)} %param.27) | copy-start | bytes 12292
  145.7 30.9 %all-to-all-start.1 = ((bf16[16,256,128]{2,1,0:T(8,128)(2,1)}), bf16[16,256,128]{2,1,0:T(8,128)(2,1)S(1)}, u32[]{:S(2)}, u32[]{:S(2)}) async-start(bf16[16,256,128]{2,1,0:T(8,128)(2,1)} %broadcast_in_dim.52), calls=%async_computation.1 | async-start | bytes 2097152 | tf_op jit(solution)/shard_map/all_to_all | solution.py:54
  208.0 3.8 %collective-permute-start = (bf16[32,12,512]{2,1,0:T(8,128)(2,1)S(1)}, bf16[32,12,512]{2,1,0:T(8,128)(2,1)S(1)}, u32[]{:S(2)}, u32[]{:S(2)}) collective-permute-start(bf16[32,12,512]{2,1,0:T(8,128)(2,1)S(1)} %all_to_all.25), channel_id=1, source_target_pairs={{0,1},{1,0},{2,3},{3,2},{4,5},{5,4},{6,7},{7,6},{8,9},{9,8},{10,11... | collective-permute-start | bytes 1179656 | tf_op jit(solution)/shard_map/ppermute | solution.py:64
  213.5 21.2 %collective-permute-start.1 = (bf16[32,12,1024]{2,0,1:T(8,128)(2,1)}, bf16[32,12,1024]{2,0,1:T(8,128)(2,1)}, u32[]{:S(2)}, u32[]{:S(2)}) collective-permute-start(bf16[32,12,1024]{2,0,1:T(8,128)(2,1)} %copy.73), channel_id=1, source_target_pairs={{0,2},{1,3},{2,0},{3,1},{4,6},{5,7},{6,4},{7,5},{8,10},{9,11},{10,... | collective-permute-start | bytes 2359304 | tf_op jit(solution)/shard_map/ppermute | solution.py:64
  237.3 2.8 copy-start.2
  253.1 20.1 %collective-permute-start.2 = (bf16[384,4,2,128]{3,1,0,2:T(4,128)(2,1)S(1)}, bf16[384,4,2,128]{3,1,0,2:T(4,128)(2,1)}, u32[]{:S(2)}, u32[]{:S(2)}) collective-permute-start(bf16[384,4,2,128]{3,1,0,2:T(4,128)(2,1)S(1)} %bitcast.310), channel_id=1, source_target_pairs={{0,2},{1,3},{2,0},{3,1},{4,6},{5,7},{6,4},{7,5},{8,10},{9,11},{10,... | collective-permute-start | bytes 2359304 | tf_op jit(solution)/shard_map/ppermute | solution.py:64
  274.9 1.2 copy-start.1
  276.1 11.8 %copy-start.15 = (f32[256,4]{0,1:T(4,128)S(1)}, f32[256,4]{0,1:T(4,128)}, u32[]{:S(2)}) copy-start(f32[256,4]{0,1:T(4,128)} %param.29) | copy-start | bytes 12292
  276.1 12.6 %copy-start.7 = (bf16[2048,32]{0,1:T(8,128)(2,1)S(1)}, bf16[2048,32]{0,1:T(8,128)(2,1)}, u32[]{:S(2)}) copy-start(bf16[2048,32]{0,1:T(8,128)(2,1)} %param.33) | copy-start | bytes 393220
  276.2 5.1 %collective-permute-start.3 = (bf16[384,4,1,128]{3,1,0,2:T(4,128)(2,1)S(1)}, bf16[384,4,1,128]{3,1,0,2:T(4,128)(2,1)S(1)}, u32[]{:S(2)}, u32[]{:S(2)}) collective-permute-start(bf16[384,4,1,128]{3,1,0,2:T(4,128)(2,1)S(1)} %dynamic-slice_convert_fusion), channel_id=1, source_target_pairs={{0,1},{1,0},{2,3},{3,2},{4,5},{5,4},{6,7},{7,6},{8,9},{9,8},{10,11... | collective-permute-start | bytes 1179656 | tf_op jit(solution)/shard_map/ppermute | solution.py:64
  283.4 18.3 %all-to-all-start.3 = ((bf16[32,12,4,128]{3,2,1,0:T(4,128)(2,1)}), bf16[32,12,4,128]{3,2,1,0:T(4,128)(2,1)S(1)}, u32[]{:S(2)}, u32[]{:S(2)}) async-start(bf16[32,12,4,128]{3,2,1,0:T(4,128)(2,1)} %bitcast.65), calls=%async_computation.3 | async-start | bytes 786432 | tf_op jit(solution)/shard_map/all_to_all | solution.py:246
  305.2 7.1 %copy-start.8 = (bf16[2048,32]{0,1:T(8,128)(2,1)S(1)}, bf16[2048,32]{0,1:T(8,128)(2,1)}, u32[]{:S(2)}) copy-start(bf16[2048,32]{0,1:T(8,128)(2,1)} %param.34) | copy-start | bytes 393220
  305.2 7.1 %copy-start.9 = (f32[256,32]{0,1:T(8,128)S(1)}, f32[256,32]{0,1:T(8,128)}, u32[]{:S(2)}) copy-start(f32[256,32]{0,1:T(8,128)} %fusion.143) | copy-start | bytes 98308
  308.0 26.6 %copy-start.11 = (bf16[512,128]{1,0:T(8,128)(2,1)S(1)}, bf16[512,128]{1,0:T(8,128)(2,1)}, u32[]{:S(2)}) copy-start(bf16[512,128]{1,0:T(8,128)(2,1)} %param.35) | copy-start | bytes 393220
  308.0 32.8 %copy-start.4 = (bf16[256,128]{1,0:T(8,128)(2,1)S(1)}, bf16[256,128]{1,0:T(8,128)(2,1)}, u32[]{:S(2)}) copy-start(bf16[256,128]{1,0:T(8,128)(2,1)} %copy-done.3) | copy-start | bytes 196612
  308.1 24.5 %collective-permute-start.4 = (bf16[256,2,128]{2,0,1:T(8,128)(2,1)S(1)}, bf16[256,2,128]{2,0,1:T(8,128)(2,1)S(1)}, u32[]{:S(2)}, u32[]{:S(2)}) collective-permute-start(bf16[256,2,128]{2,0,1:T(8,128)(2,1)S(1)} %fusion.50), channel_id=1, source_target_pairs={{0,8},{1,9},{2,10},{3,11},{4,12},{5,13},{6,14},{7,15},{8,0},{9,1},... | collective-permute-start | bytes 393224 | tf_op jit(solution)/shard_map/ppermute | solution.py:64
  332.7 8.1 %collective-permute-start.5 = (bf16[256,1,128]{2,0,1:T(8,128)(2,1)S(1)}, bf16[256,1,128]{2,0,1:T(8,128)(2,1)S(1)}, u32[]{:S(2)}, u32[]{:S(2)}) collective-permute-start(bf16[256,1,128]{2,0,1:T(8,128)(2,1)S(1)} %dynamic-slice_convert_fusion.2), channel_id=1, source_target_pairs={{0,4},{1,5},{2,6},{3,7},{4,0},{5,1},{6,2},{7,3},{8,12},{9,13},{10,... | collective-permute-start | bytes 196616 | tf_op jit(solution)/shard_map/ppermute | solution.py:64
